TPU v7x, 32 devices: a whole 2x2x4 slice. The times are simulated.
32 devices in a mesh: sp: 8 (over z, y), tp: 4 (over x, core).
Axes of the slice: x: 2, y: 2, z: 4, core: 2. Of those that a mesh axis runs over, the one named last changes fastest.
Arguments:
- tokens: bfloat16 [2048, 2048], P(('sp', 'tp')), may hold values from -16 to 16
- w_query: bfloat16 [2048, 1024], P(None, 'tp'), may hold values from -1 to 1
- w_key: bfloat16 [2048, 256], P(None, 'tp'), may hold values from -1 to 1
- w_value: bfloat16 [2048, 256], P(None, 'tp'), may hold values from -0.125 to 0.125
- w_gate: bfloat16 [2048, 16], P(None, 'tp'), may hold values from -0.125 to 0.125
- gate_bias: float32 [16], P('tp'), as said below
- w_output: bfloat16 [1024, 2048], P('tp'), may hold values from -0.1875 to 0.1875
Outputs:
- mixed: bfloat16 [2048, 2048], P(('sp', 'tp'))
Inputs may be any that keep to these rules, and one draw needn't show every extreme that they name: `gate_bias`: each head's forget gate bias is 4 or more; there is no upper bound.
All inputs are finite; a program needn't handle non-finite values.
Results may differ from a plain program's by a relative error of at most 0.012.
The roundings to bfloat16 on the way count: a program that leaves them out, or rounds other values in their place, can miss the bound.
Values may be sent and summed in bfloat16 or wider, within the bound.
A program may use at most 64 MiB of HBM per device.

v0:
```python
import math

import jax
import jax.numpy as jnp
from jax import lax
from jax.sharding import PartitionSpec as P

HEAD = 64


masked_value = -1e30


def softmax_update(
    carry_state,
    query_here,
    query_cumul,
    query_position,
    key_here,
    value_here,
    key_cumul,
    key_position,
):
    row_peak, row_mass, row_accum = carry_state
    scores = jnp.einsum(
        "kgtd,skd->kgts", query_here, key_here, preferred_element_type=jnp.float32
    ) * HEAD ** (-0.5)
    scores = scores + query_cumul[:, :, :, None] - key_cumul[:, :, None, :]
    allowed = key_position[None, :] <= query_position[:, None]
    scores = jnp.where(allowed, scores, masked_value)
    new_peak = jnp.maximum(row_peak, jnp.max(scores, axis=3))
    weights = jnp.where(allowed, jnp.exp(scores - new_peak[:, :, :, None]), 0.0)
    rescale = jnp.exp(row_peak - new_peak)
    row_mass = row_mass * rescale + jnp.sum(weights, axis=3)
    row_accum = row_accum * rescale[:, :, :, None] + jnp.einsum(
        "kgts,skd->kgtd",
        weights.astype(jnp.bfloat16),
        value_here,
        preferred_element_type=jnp.float32,
    )
    return (new_peak, row_mass, row_accum)


def shards(tokens, w_query, w_key, w_value, w_gate, gate_bias, w_output):
    sp_count = lax.axis_size("sp")
    sp_rank = lax.axis_index("sp")
    query_cols = w_query.shape[1]
    key_cols = w_key.shape[1]
    heads_here = w_gate.shape[1]
    kv_heads_here = key_cols // HEAD
    group_size = heads_here // kv_heads_here
    joined = jnp.concatenate([w_query, w_key, w_value, w_gate], axis=1)
    projected = jnp.dot(
        lax.all_gather(tokens, "tp", axis=0, tiled=True), joined, preferred_element_type=jnp.float32
    ).astype(jnp.bfloat16)
    local_rows = projected.shape[0]
    half_rows = local_rows // 2
    second_block = 2 * sp_rank + 1
    own_gates = jax.nn.log_sigmoid(
        projected[:, query_cols + 2 * key_cols :].astype(jnp.float32) + gate_bias
    )
    totals = jnp.sum(own_gates.reshape(2, half_rows, heads_here), axis=1)
    all_totals = lax.all_gather(totals[None], "sp", axis=0, tiled=True)
    ordered = all_totals.reshape(2 * sp_count, heads_here)
    prefix_sums = jnp.cumsum(ordered, axis=0) - ordered
    queries = (
        projected[:, :query_cols]
        .reshape(2, half_rows, kv_heads_here, group_size, HEAD)
        .transpose(0, 2, 3, 1, 4)
    )
    query_blocks = (2 * sp_rank, second_block)
    query_cumul = []
    query_position = []
    for side_index in range(2):
        base_value = lax.dynamic_index_in_dim(
            prefix_sums, query_blocks[side_index], 0, keepdims=False
        )
        cumul_rows = base_value[None, :] + jnp.cumsum(
            own_gates[side_index * half_rows : (side_index + 1) * half_rows], axis=0
        )
        query_cumul.append(
            cumul_rows.reshape(half_rows, kv_heads_here, group_size).transpose(1, 2, 0)
        )
        query_position.append(
            query_blocks[side_index] * half_rows + jnp.arange(half_rows, dtype=jnp.int32)
        )
    initial = (
        jnp.full((2, kv_heads_here, group_size, half_rows), masked_value, jnp.float32),
        jnp.zeros((2, kv_heads_here, group_size, half_rows), jnp.float32),
        jnp.zeros((2, kv_heads_here, group_size, half_rows, HEAD), jnp.float32),
    )
    gathered = lax.all_gather(projected[:, query_cols:], "sp", axis=0, tiled=True)
    row_count = gathered.shape[0]
    piece_blocks = row_count // half_rows
    per_step = math.gcd(piece_blocks, max(1, 1024 // half_rows))
    step_rows = per_step * half_rows
    step_count = row_count // step_rows
    first_row = half_rows * jnp.arange(piece_blocks, dtype=jnp.int32)
    owner_rank = first_row // local_rows
    half_index = first_row % local_rows // half_rows
    block_ids = 2 * owner_rank + half_index
    gate_logs = jax.nn.log_sigmoid(gathered[:, 2 * key_cols :].astype(jnp.float32) + gate_bias)
    gate_logs = gate_logs.reshape(piece_blocks, half_rows, heads_here)
    base_values = jnp.take(prefix_sums, block_ids, axis=0)
    key_cumul_all = (base_values[:, None, :] + jnp.cumsum(gate_logs, axis=1)).reshape(
        row_count, kv_heads_here, group_size
    )
    key_position_all = (
        block_ids[:, None] * half_rows + jnp.arange(half_rows, dtype=jnp.int32)[None, :]
    ).reshape(row_count)
    earliest = jnp.min(block_ids.reshape(step_count, per_step), axis=1)

    def one_step(step_index, inner_state):
        start_row = step_index * step_rows
        block_rows = lax.dynamic_slice_in_dim(gathered, start_row, step_rows, 0)
        key_here = block_rows[:, :key_cols].reshape(step_rows, kv_heads_here, HEAD)
        value_here = block_rows[:, key_cols : 2 * key_cols].reshape(step_rows, kv_heads_here, HEAD)
        key_cumul = lax.dynamic_slice_in_dim(key_cumul_all, start_row, step_rows, 0).transpose(
            1, 2, 0
        )
        key_position = lax.dynamic_slice_in_dim(key_position_all, start_row, step_rows, 0)
        first_id = earliest[step_index]
        results = []
        for side_index in range(2):
            head_state = tuple((member[side_index] for member in inner_state))

            def compute(head_state, side_index=side_index):
                return softmax_update(
                    head_state,
                    queries[side_index],
                    query_cumul[side_index],
                    query_position[side_index],
                    key_here,
                    value_here,
                    key_cumul,
                    key_position,
                )

            head_state = lax.cond(
                first_id <= query_blocks[side_index],
                compute,
                lambda unchanged: unchanged,
                head_state,
            )
            results.append(head_state)
        return tuple((jnp.stack([results[0][member], results[1][member]]) for member in range(3)))

    row_peak, row_mass, row_accum = lax.fori_loop(0, step_count, one_step, initial)
    attended = (row_accum / row_mass[:, :, :, :, None]).astype(jnp.bfloat16)
    attended = attended.transpose(0, 3, 1, 2, 4).reshape(local_rows, heads_here * HEAD)
    return lax.psum_scatter(
        jnp.dot(attended, w_output, preferred_element_type=jnp.float32).astype(jnp.bfloat16),
        "tp",
        scatter_dimension=0,
        tiled=True,
    )


def solution(mesh):
    return jax.shard_map(
        shards,
        mesh=mesh,
        in_specs=(
            P(("sp", "tp"), None),
            P(None, "tp"),
            P(None, "tp"),
            P(None, "tp"),
            P(None, "tp"),
            P("tp"),
            P("tp", None),
        ),
        out_specs=P(("sp", "tp"), None),
        check_vma=False,
    )
```

profile of v0, /device:TPU:17, one launch (start us, length us, event | category | flops | bytes accessed | tf_op | source)
XLA Modules:
  0.0 128.9 jit_solution(12914409057158961123)
XLA Ops:
  6.5 0.7 all-gather.4.cloned.1.call-update
  7.3 1.0 copy.42
  8.3 1.2 copy.41
  9.6 1.2 copy.40
  11.1 16.0 %all-gather.4.cloned.1.call-done = bf16[256,2048]{1,0:T(8,128)(2,1)} async-done(((bf16[64,2048]{1,0:T(8,128)(2,1)}), bf16[256,2048]{1,0:T(8,128)(2,1)}) %all-gather.4.cloned.1.call-update) | async-done | bytes 1048592 | tf_op jit(solution)/shard_map/all_gather | solution.py:54
  27.1 2.7 %fusion.47 = bf16[256,388]{0,1:T(8,128)(2,1)S(1)} fusion(bf16[256,2048]{1,0:T(8,128)(2,1)} %all-gather.4.cloned.1.call-done, bf16[2048,4]{1,0:T(8,128)(2,1)S(1)} %copy.42, bf16[2048,64]{1,0:T(8,128)(2,1)S(1)} %copy.41, bf16[2048,64]{1,0:T(8,128)(2,1)S(1)} %copy.40, bf16[2048,256]{1,0:T(8,128)(2,1)} %param.14), kind=kOutput, calls=%fused_computation.71 | convolution fusion | flops 413303808 | bytes 2836480 | tf_op jit(solution)/shard_map/dot_general | solution.py:53
  30.0 21.2 %all_gather.10 = bf16[2048,132]{0,1:T(8,128)(2,1)S(1)} all-gather(bf16[256,132]{0,1:T(8,128)(2,1)S(1)} %slice.96), channel_id=1, replica_groups=mesh['sp'=8,'tp'=4] {'sp'}, dimensions={0}, use_global_device_ids=true | all-gather | bytes 608256 | tf_op jit(solution)/shard_map/all_gather | solution.py:92
  51.3 15.9 %all-gather.1 = f32[8,2,4]{2,1,0:T(2,128)S(1)} all-gather(f32[1,2,4]{2,1,0:T(2,128)S(1)} %bitcast.194), channel_id=2, replica_groups=mesh['sp'=8,'tp'=4] {'sp'}, dimensions={0}, use_global_device_ids=true | all-gather | bytes 288 | tf_op jit(solution)/shard_map/all_gather | solution.py:63
  68.5 1.2 broadcast_add_fusion.2
  69.7 1.6 %copy.45 = f32[16,128,4]{1,0,2:T(8,128)S(1)} copy(f32[16,128,4]{2,0,1:T(8,128)} %broadcast_add_fusion.2) | data formatting | bytes 65536 | tf_op jit(solution)/shard_map/add | solution.py:105
  72.2 13.3 %while.18 = (s32[]{:T(128)}, f32[2,1,4,128]{3,2,1,0:T(4,128)S(1)}, f32[2,1,4,128]{3,2,1,0:T(4,128)S(1)}, f32[2,1,4,128,64]{3,4,2,1,0:T(8,128)S(1)}, s32[2]{0:T(1...) while((s32[]{:T(128)}, f32[2,1,4,128]{3,2,1,0:T(4,128)S(1)}, ...), condition=%wide.region_15.16_spmd.clone, body=%wide.region_6.15_spmd.clone.sunk | while | flops 280433920 | bytes 16568903 | solution.py:148
  72.2 0.7 dynamic_slice.54
  73.7 2.2 %conditional.6 = (f32[1,1,4,128]{3,2,1,0:T(4,128)S(1)}, f32[1,1,4,128]{3,2,1,0:T(4,128)S(1)}, f32[1,1,4,128,64]{3,4,2,1,0:T(8,128)S(1)}) conditional(s32[]{:T(128)} %convert_element_type.63, (f32[1,4,128]{2,1,0:T(4,128)S(1)}, f32[1,4,128]{2,1,0:T(4,128)S(1)}, f32[1,4,128,64]{2,3,1,0:T(8,128)S(1)}) %tuple.137, (s32[1024]{0:T(1024)S(1)}, s32[]{:T(128)}, ...), branch_computations={%region_11.11_spmd, %region_12.14_spmd} | conditional | flops 140183168 | bytes 7460380 | solution.py:139
  73.9 0.8 fusion.60
  76.6 2.2 %conditional.7 = (f32[1,1,4,128]{3,2,1,0:T(4,128)S(1)}, f32[1,1,4,128]{3,2,1,0:T(4,128)S(1)}, f32[1,1,4,128,64]{3,4,2,1,0:T(8,128)S(1)}) conditional(s32[]{:T(128)} %convert_element_type.64, (f32[1,4,128]{2,1,0:T(4,128)S(1)}, f32[1,4,128]{2,1,0:T(4,128)S(1)}, f32[1,4,128,64]{2,3,1,0:T(8,128)S(1)}) %tuple.139, (s32[1024]{0:T(1024)S(1)}, s32[]{:T(128)}, ...), branch_computations={%region_7.7_spmd, %region_8.10_spmd} | conditional | flops 140183168 | bytes 7460380 | solution.py:139
  76.8 0.8 fusion.59
  78.9 0.7 dynamic_slice.54
  80.4 2.2 %conditional.6 = (f32[1,1,4,128]{3,2,1,0:T(4,128)S(1)}, f32[1,1,4,128]{3,2,1,0:T(4,128)S(1)}, f32[1,1,4,128,64]{3,4,2,1,0:T(8,128)S(1)}) conditional(s32[]{:T(128)} %convert_element_type.63, (f32[1,4,128]{2,1,0:T(4,128)S(1)}, f32[1,4,128]{2,1,0:T(4,128)S(1)}, f32[1,4,128,64]{2,3,1,0:T(8,128)S(1)}) %tuple.137, (s32[1024]{0:T(1024)S(1)}, s32[]{:T(128)}, ...), branch_computations={%region_11.11_spmd, %region_12.14_spmd} | conditional | flops 140183168 | bytes 7460380 | solution.py:139
  80.6 0.8 fusion.60
  83.3 2.2 %conditional.7 = (f32[1,1,4,128]{3,2,1,0:T(4,128)S(1)}, f32[1,1,4,128]{3,2,1,0:T(4,128)S(1)}, f32[1,1,4,128,64]{3,4,2,1,0:T(8,128)S(1)}) conditional(s32[]{:T(128)} %convert_element_type.64, (f32[1,4,128]{2,1,0:T(4,128)S(1)}, f32[1,4,128]{2,1,0:T(4,128)S(1)}, f32[1,4,128,64]{2,3,1,0:T(8,128)S(1)}) %tuple.139, (s32[1024]{0:T(1024)S(1)}, s32[]{:T(128)}, ...), branch_computations={%region_7.7_spmd, %region_8.10_spmd} | conditional | flops 140183168 | bytes 7460380 | solution.py:139
  83.5 0.8 fusion.59
  84.9 0.6 fusion.7
  85.7 1.5 %convolution_convert_fusion = bf16[256,2048]{1,0:T(8,128)(2,1)} fusion(bf16[256,2048]{1,0:T(8,128)(2,1)S(1)} %copy-done, bf16[32,8,2,128]{3,2,1,0:T(2,128)(2,1)S(1)} %bitcast.184), kind=kOutput, calls=%fused_computation.61 | convolution fusion | flops 268959744 | bytes 2228224 | tf_op jit(solution)/shard_map/dot_general | solution.py:152
  87.2 34.9 %reduce-scatter.2.cloned.1.call-done = bf16[64,2048]{1,0:T(8,128)(2,1)} async-done(((bf16[256,2048]{1,0:T(8,128)(2,1)}), bf16[64,2048]{1,0:T(8,128)(2,1)}) %reduce-scatter.2.cloned.1.call-update) | async-done | bytes 262160 | tf_op jit(solution)/shard_map/reduce_scatter | solution.py:151
  (86 shorter events, 8.1 us)
Async XLA Ops:
  6.5 79.2 %copy-start = (bf16[256,2048]{1,0:T(8,128)(2,1)S(1)}, bf16[256,2048]{1,0:T(8,128)(2,1)}, u32[]{:S(2)}) copy-start(bf16[256,2048]{1,0:T(8,128)(2,1)} %param.19) | copy-start | bytes 3145732
  6.5 20.5 %all-gather.4.cloned.1.call-start = ((), (), s32[]{:S(2)}) async-start(), calls=%async_computation.1 | async-start | bytes 1310720 | tf_op jit(solution)/shard_map/all_gather | solution.py:54
  7.3 114.8 %reduce-scatter.2.cloned.1.call-start = ((), (), s32[]{:S(2)}) async-start(), calls=%async_computation.2 | async-start | bytes 1310720 | tf_op jit(solution)/shard_map/reduce_scatter | solution.py:151
  11.1 18.7 %copy-start.1 = (f32[4]{0:T(128)S(1)}, f32[4]{0:T(128)}, u32[]{:S(2)}) copy-start(f32[4]{0:T(128)} %param.18) | copy-start | bytes 52
Sparse Core Ops, SparseCore 0:
  8.9 18.1 all-gather.3
  87.3 34.6 reduce-scatter.1
where the time goes:
time: 131 us; the launch traced here: 129 us
  waiting for transfers between devices  51.5 us (39%)
  blocking collectives  37 us (28%)
  between operations  13.6 us (10%)
  matrix products  9.72 us (7%)
  local copies, waits for them, and re-layouts  8.46 us (6%)
  other arithmetic  5.36 us (4%)
  loops' own time  3.16 us (2%)
    reduce_scatter x1, waiting for transfers between devices, shards(): lax.psum_scatter(jnp.dot(attended, w_output, preferred_element_type=jnp.f...  34.9 us
    all_gather x1, blocking collectives, shards(): lax.all_gather(projected[:, query_cols:], 'sp', axis=0, tiled=True)  21.2 us
    all_gather x1, waiting for transfers between devices, shards(): lax.all_gather(tokens, 'tp', axis=0, tiled=True)  16 us
    all_gather x1, blocking collectives, shards(): all_totals = lax.all_gather(totals[None], 'sp', axis=0, tiled=True)  15.9 us
    unnamed x10, local copies, waits for them, and re-layouts  3.63 us
    dot_general x4, matrix products, softmax_update(): jnp.einsum('kgtd,skd->kgts', query_here, key_here, preferred_element_type...  3.08 us
    another operation x1, loops' own time, shards(): lax.fori_loop(0, step_count, one_step, initial)  3.02 us
    dot_general x1, matrix products, shards(): jnp.dot(lax.all_gather(tokens, 'tp', axis=0, tiled=True), joined, preferr...  2.71 us
  transfers between devices with their start and end apart: 2, of which 2 were waited for; matrix products, arithmetic and copies ran while one was open for 3% of the time, Pallas kernels for 0%

commit v1 on v0

v1 whole, which is shorter than its diff:
```python
import functools

import jax
import jax.numpy as jnp
from jax import lax
from jax.experimental import pallas as pl
from jax.experimental.pallas import tpu as pltpu
from jax.sharding import PartitionSpec as P

HEAD = 64
LANES = 128
masked_value = -1e30
MESH = pl.DeviceIdType.MESH


def kernel(
    sp, tp, chunks, out_chunks,
    tokens, w_query, w_key, w_value, w_gate, bias, w_output,
    out,
    tok, w_all, w_k, w_v, w_g, wo, wo_pair, proj, qs, kv, cum,
    peak, mass, accum, att, att_pair, keep, outgoing, incoming,
    local_sem, own_sem, cross_send, cross_recv, pair_send, pair_recv, relay_send, relay_recv,
    wo_send, wo_recv, kv_send, kv_recv, cum_send, cum_recv,
    att_send, att_recv, out_send, out_recv,
):
    lo_n = 2
    hi_n = tp // lo_n
    me = lax.axis_index("sp")
    t_me = lax.axis_index("tp")
    hi, lo = lax.div(t_me, lo_n), lax.rem(t_me, lo_n)
    pair = hi * lo_n + (1 - lo)
    rows = tok.shape[1]
    local_rows = rows * tp
    width = tok.shape[2]
    q_cols = w_query.shape[1]
    heads = w_gate.shape[1]
    key_cols = w_key.shape[1]
    piece = width // chunks
    out_cols = w_output.shape[1]
    out_piece = out_cols // out_chunks

    def cross(d):
        return lax.rem(hi + d, hi_n) * lo_n + lo

    loads = [
        pltpu.make_async_copy(w_key, w_k, local_sem.at[0]),
        pltpu.make_async_copy(w_value, w_v, local_sem.at[1]),
        pltpu.make_async_copy(w_gate, w_g, local_sem.at[2]),
        pltpu.make_async_copy(w_query, w_all.at[:, pl.ds(0, q_cols)], local_sem.at[3]),
        pltpu.make_async_copy(w_output, wo, local_sem.at[4]),
    ]
    own = pltpu.make_async_copy(tokens, tok.at[t_me], own_sem)
    own.start()
    for load in loads:
        load.start()

    barrier = pltpu.get_barrier_semaphore()
    pl.semaphore_signal(barrier, inc=1, device_id={"tp": pair}, device_id_type=MESH)
    for d in range(1, hi_n):
        pl.semaphore_signal(barrier, inc=1, device_id={"tp": cross(d)}, device_id_type=MESH)

    def greet(d, carry):
        pl.semaphore_signal(
            barrier, inc=1, device_id={"sp": lax.rem(me + d, sp)}, device_id_type=MESH
        )
        return carry

    lax.fori_loop(1, sp, greet, 0)
    pl.semaphore_wait(barrier, 1 + (hi_n - 1) + (sp - 1))

    def cols(k):
        return pl.ds(k * piece, piece)

    def cross_copy(d, k):
        return pltpu.make_async_remote_copy(
            tokens.at[:, cols(k)], tok.at[t_me, :, cols(k)],
            cross_send.at[d - 1, k], cross_recv.at[d - 1, k],
            device_id={"tp": cross(d)}, device_id_type=MESH,
        )

    def pair_copy(k):
        return pltpu.make_async_remote_copy(
            tokens.at[:, cols(k)], tok.at[t_me, :, cols(k)],
            pair_send.at[k], pair_recv.at[k],
            device_id={"tp": pair}, device_id_type=MESH,
        )

    def relay_copy(d, k):
        source = lax.rem(hi - d + hi_n, hi_n) * lo_n + lo
        return pltpu.make_async_remote_copy(
            tok.at[source, :, cols(k)], tok.at[source, :, cols(k)],
            relay_send.at[d - 1, k], relay_recv.at[d - 1, k],
            device_id={"tp": pair}, device_id_type=MESH,
        )

    for k in range(chunks):
        for d in range(1, hi_n):
            cross_copy(d, k).start()
    for k in range(chunks):
        pair_copy(k).start()

    for load in loads[:3]:
        load.wait()
    build = 256

    def assemble(i, carry):
        span = pl.ds(pl.multiple_of(i * build, build), build)
        w_all[span, q_cols:q_cols + LANES] = jnp.concatenate([w_k[span, :], w_v[span, :]], axis=1)
        w_all[span, q_cols + LANES:] = jnp.concatenate(
            [w_g[span, :], jnp.zeros((build, LANES - heads), jnp.bfloat16)], axis=1
        )
        return carry

    lax.fori_loop(0, width // build, assemble, 0)
    loads[3].wait()
    loads[4].wait()
    own.wait()
    wo_copy = pltpu.make_async_remote_copy(
        wo, wo_pair, wo_send, wo_recv, device_id={"tp": pair}, device_id_type=MESH
    )

    for k in range(chunks):
        for d in range(1, hi_n):
            cross_copy(d, k).wait_recv()
            relay_copy(d, k).start()
        pair_copy(k).wait_recv()
        for d in range(1, hi_n):
            relay_copy(d, k).wait_recv()
        here = tok[:, :, k * piece:(k + 1) * piece].reshape(local_rows, piece)
        part = jnp.dot(here, w_all[k * piece:(k + 1) * piece, :], preferred_element_type=jnp.float32)
        if k == 0:
            proj[...] = part
        else:
            proj[...] += part
    wo_copy.start()

    kv[me] = proj[:, q_cols:q_cols + 2 * key_cols].astype(jnp.bfloat16)
    scale = HEAD ** -0.5
    for h in range(heads):
        q = proj[:, h * HEAD:(h + 1) * HEAD].astype(jnp.bfloat16) * jnp.bfloat16(scale)
        qs[h] = jnp.concatenate([q, jnp.zeros((local_rows, LANES - HEAD), jnp.bfloat16)], axis=1)

    def kv_copy(d):
        return pltpu.make_async_remote_copy(
            kv.at[me], kv.at[me], kv_send.at[d], kv_recv.at[me],
            device_id={"sp": d}, device_id_type=MESH,
        )

    def cum_copy(d):
        return pltpu.make_async_remote_copy(
            cum.at[me], cum.at[me], cum_send.at[d], cum_recv.at[me],
            device_id={"sp": d}, device_id_type=MESH,
        )

    def arrival(r):
        return (
            pltpu.make_async_remote_copy(
                kv.at[r], kv.at[r], kv_send.at[r], kv_recv.at[r],
                device_id={"sp": r}, device_id_type=MESH,
            ),
            pltpu.make_async_remote_copy(
                cum.at[r], cum.at[r], cum_send.at[r], cum_recv.at[r],
                device_id={"sp": r}, device_id_type=MESH,
            ),
        )

    later = sp - 1 - me

    def send_kv(i, carry):
        kv_copy(sp - 1 - i).start()
        return carry

    def send_cum(i, carry):
        cum_copy(sp - 1 - i).start()
        return carry

    lax.fori_loop(0, later, send_kv, 0)

    logits = proj[:, q_cols + LANES:].astype(jnp.bfloat16).astype(jnp.float32).T[:8, :]
    u = logits + bias[...]
    gates = jnp.minimum(u, 0.0) - jnp.log1p(jnp.exp(-jnp.abs(u)))
    upper = (
        lax.broadcasted_iota(jnp.int32, (local_rows, local_rows), 0)
        <= lax.broadcasted_iota(jnp.int32, (local_rows, local_rows), 1)
    )
    ones = jnp.where(upper, 1.0, 0.0).astype(jnp.bfloat16)
    g0 = gates.astype(jnp.bfloat16)
    r1 = gates - g0.astype(jnp.float32)
    g1 = r1.astype(jnp.bfloat16)
    g2 = (r1 - g1.astype(jnp.float32)).astype(jnp.bfloat16)
    total = jnp.dot(g2, ones, preferred_element_type=jnp.float32)
    total = total + jnp.dot(g1, ones, preferred_element_type=jnp.float32)
    total = total + jnp.dot(g0, ones, preferred_element_type=jnp.float32)
    cum[me] = total
    lax.fori_loop(0, later, send_cum, 0)

    halves = local_rows // LANES

    def lane_parts(x):
        return [x[:, j * LANES:(j + 1) * LANES] for j in range(halves)]

    def attend(h, kv_here, bias_row, first):
        s = lax.dot_general(
            qs[h], kv_here, (((1,), (1,)), ((), ())), preferred_element_type=jnp.float32
        ) + bias_row
        if first:
            allowed = (
                lax.broadcasted_iota(jnp.int32, (local_rows, local_rows), 1)
                <= lax.broadcasted_iota(jnp.int32, (local_rows, local_rows), 0)
            )
            s = jnp.where(allowed, s, masked_value)
        top = jnp.max(s, axis=1, keepdims=True)
        if first:
            new_peak = jnp.broadcast_to(top, (local_rows, LANES))
        else:
            old_peak = peak[h]
            new_peak = jnp.maximum(old_peak, top)
        p = [jnp.exp(x - new_peak) for x in lane_parts(s)]
        p_sum = functools.reduce(lambda a, b: a + b, p)
        weights = jnp.concatenate([x.astype(jnp.bfloat16) for x in p], axis=1)
        term = jnp.dot(weights, kv_here, preferred_element_type=jnp.float32)
        peak[h] = new_peak
        if first:
            mass[h] = p_sum
            accum[h] = term
        else:
            rescale = jnp.exp(old_peak - new_peak)
            mass[h] = mass[h] * rescale + p_sum
            accum[h] = accum[h] * rescale + term

    for h in range(heads):
        attend(h, kv[me], -total[h:h + 1, :], True)

    def one_block(i, base):
        r = me - 1 - i
        for copy in arrival(r):
            copy.wait_recv()
        cum_here = cum[r]
        base = base + cum_here[:, local_rows - 1:]
        shift = base - cum_here
        kv_here = kv[r]
        for h in range(heads):
            attend(h, kv_here, shift[h:h + 1, :], False)
        return base

    lax.fori_loop(0, me, one_block, jnp.zeros((8, 1), jnp.float32))

    for h in range(heads):
        denominator = jnp.sum(mass[h], axis=1, keepdims=True)
        done = (accum[h][:, key_cols:2 * key_cols] / denominator).astype(jnp.bfloat16)
        att[:, :, :, h * HEAD:(h + 1) * HEAD] = done.reshape(hi_n, lo_n, rows, HEAD)

    def att_copy(d):
        return pltpu.make_async_remote_copy(
            att.at[d, 1 - lo], att_pair.at[d], att_send.at[d], att_recv.at[d],
            device_id={"tp": pair}, device_id_type=MESH,
        )

    for d in range(hi_n):
        att_copy(d).start()
    wo_copy.wait_recv()
    for d in range(hi_n):
        att_copy(d).wait_recv()
    mine = att[:, lo].reshape(hi_n * rows, q_cols)
    theirs = att_pair[...].reshape(hi_n * rows, q_cols)

    def out_copy(d, k):
        span = pl.ds(k * out_piece, out_piece)
        return pltpu.make_async_remote_copy(
            outgoing.at[lax.rem(hi + d, hi_n), :, span], incoming.at[d - 1, :, span],
            out_send.at[d - 1, k], out_recv.at[d - 1, k],
            device_id={"tp": cross(d)}, device_id_type=MESH,
        )

    for k in range(out_chunks):
        span = slice(k * out_piece, (k + 1) * out_piece)
        a = jnp.dot(mine, wo[:, span], preferred_element_type=jnp.float32).astype(jnp.bfloat16)
        b = jnp.dot(theirs, wo_pair[:, span], preferred_element_type=jnp.float32).astype(jnp.bfloat16)
        both = a.astype(jnp.float32) + b.astype(jnp.float32)
        keep[:, :, span] = both.reshape(hi_n, rows, out_piece)
        outgoing[:, :, span] = both.astype(jnp.bfloat16).reshape(hi_n, rows, out_piece)
        for d in range(1, hi_n):
            out_copy(d, k).start()
    for k in range(out_chunks):
        span = slice(k * out_piece, (k + 1) * out_piece)
        value = keep[hi, :, span]
        for d in range(1, hi_n):
            out_copy(d, k).wait_recv()
            value = value + incoming[d - 1, :, span].astype(jnp.float32)
        out[:, span] = value.astype(jnp.bfloat16)

    for k in range(chunks):
        for d in range(1, hi_n):
            cross_copy(d, k).wait_send()
            relay_copy(d, k).wait_send()
        pair_copy(k).wait_send()
    wo_copy.wait_send()
    for d in range(hi_n):
        att_copy(d).wait_send()
    for k in range(out_chunks):
        for d in range(1, hi_n):
            out_copy(d, k).wait_send()

    def drain(i, carry):
        kv_copy(sp - 1 - i).wait_send()
        cum_copy(sp - 1 - i).wait_send()
        return carry

    lax.fori_loop(0, later, drain, 0)


def shards(tokens, w_query, w_key, w_value, w_gate, gate_bias, w_output):
    sp = lax.axis_size("sp")
    tp = lax.axis_size("tp")
    rows, width = tokens.shape
    local_rows = rows * tp
    q_cols, key_cols, heads = w_query.shape[1], w_key.shape[1], w_gate.shape[1]
    out_cols = w_output.shape[1]
    assert tp % 2 == 0 and 2 * key_cols == LANES and key_cols == HEAD and heads <= 8
    hi_n = tp // 2
    chunks = 4
    out_chunks = 4
    bias = jnp.pad(gate_bias, (0, 8 - heads), constant_values=4.0)[:, None]
    bf, f32 = jnp.bfloat16, jnp.float32
    dma = pltpu.SemaphoreType.DMA
    any_spec = pl.BlockSpec(memory_space=pl.ANY)
    vmem_spec = pl.BlockSpec(memory_space=pltpu.VMEM)
    return pl.pallas_call(
        functools.partial(kernel, sp, tp, chunks, out_chunks),
        out_shape=jax.ShapeDtypeStruct((rows, out_cols), bf),
        in_specs=[any_spec] * 5 + [vmem_spec, any_spec],
        out_specs=vmem_spec,
        scratch_shapes=[
            pltpu.VMEM((tp, rows, width), bf),
            pltpu.VMEM((width, q_cols + 2 * LANES), bf),
            pltpu.VMEM(w_key.shape, bf),
            pltpu.VMEM(w_value.shape, bf),
            pltpu.VMEM(w_gate.shape, bf),
            pltpu.VMEM(w_output.shape, bf),
            pltpu.VMEM(w_output.shape, bf),
            pltpu.VMEM((local_rows, q_cols + 2 * LANES), f32),
            pltpu.VMEM((heads, local_rows, LANES), bf),
            pltpu.VMEM((sp, local_rows, LANES), bf),
            pltpu.VMEM((sp, 8, local_rows), f32),
            pltpu.VMEM((heads, local_rows, LANES), f32),
            pltpu.VMEM((heads, local_rows, LANES), f32),
            pltpu.VMEM((heads, local_rows, LANES), f32),
            pltpu.VMEM((hi_n, 2, rows, q_cols), bf),
            pltpu.VMEM((hi_n, rows, q_cols), bf),
            pltpu.VMEM((hi_n, rows, out_cols), f32),
            pltpu.VMEM((hi_n, rows, out_cols), bf),
            pltpu.VMEM((max(hi_n - 1, 1), rows, out_cols), bf),
            dma((5,)),
            dma,
            dma((hi_n - 1, chunks)),
            dma((hi_n - 1, chunks)),
            dma((chunks,)),
            dma((chunks,)),
            dma((hi_n - 1, chunks)),
            dma((hi_n - 1, chunks)),
            dma,
            dma,
            dma((sp,)),
            dma((sp,)),
            dma((sp,)),
            dma((sp,)),
            dma((hi_n,)),
            dma((hi_n,)),
            dma((hi_n - 1, out_chunks)),
            dma((hi_n - 1, out_chunks)),
        ],
        compiler_params=pltpu.CompilerParams(
            collective_id=0, has_side_effects=True, vmem_limit_bytes=56 * 1024 * 1024
        ),
    )(tokens, w_query, w_key, w_value, w_gate, bias, w_output)


def solution(mesh):
    return jax.shard_map(
        shards,
        mesh=mesh,
        in_specs=(
            P(("sp", "tp"), None),
            P(None, "tp"),
            P(None, "tp"),
            P(None, "tp"),
            P(None, "tp"),
            P("tp"),
            P("tp", None),
        ),
        out_specs=P(("sp", "tp"), None),
        check_vma=False,
    )
```

time: 131 us -> 49.2 us (0.38); the launches traced: 129 us -> 49 us
  waiting for transfers between devices: 51.5 us -> 0 us
  Pallas kernels: 0 us -> 42 us
  blocking collectives: 37 us -> 0 us
  between operations: 13.6 us -> 0.01 us
  matrix products: 9.72 us -> 0 us
  other arithmetic: 5.36 us -> 0 us
  loops' own time: 3.16 us -> 0 us
  local copies, waits for them, and re-layouts: 8.46 us -> 7.06 us
    pallas_call x0 -> x1, Pallas kernels: none -> 42 us  [shards(): pl.pallas_call(functools.partial(kernel, sp, tp, chunks, out_chunks), out...]
    all_gather x2 -> x0, blocking collectives: 37 us -> none  [the longest x1 21.2 us: shards(): lax.all_gather(projected[:, query_cols:], 'sp', axis=0, tiled=True)]
    reduce_scatter x1 -> x0, waiting for transfers between devices: 34.9 us -> none  [shards(): lax.psum_scatter(jnp.dot(attended, w_output, preferred_element_type=jnp.f...]
    all_gather x1 -> x0, waiting for transfers between devices: 16 us -> none  [shards(): lax.all_gather(tokens, 'tp', axis=0, tiled=True)]
    dot_general x10 -> x0, matrix products: 9.72 us -> none  [the longest x4 3.08 us: softmax_update(): jnp.einsum('kgtd,skd->kgts', query_here, key_here, preferred_element_type...]
    another operation x5 -> x0, loops' own time: 3.16 us -> none  [the longest x1 3.02 us: shards(): lax.fori_loop(0, step_count, one_step, initial)]
    reduce_sum x5 -> x0, other arithmetic: 2.46 us -> none  [the longest x4 2.37 us: softmax_update(): row_mass = row_mass * rescale + jnp.sum(weights, axis=3)]
    unnamed x10 -> x8, local copies, waits for them, and re-layouts: 3.63 us -> 5.73 us
  transfers between devices with their start and end apart: 2 -> 0, of which waited for: 2 -> 0; matrix products, arithmetic and copies ran while one was open for 3% -> 0% of each run, Pallas kernels for 0% -> 0%
where the time goes in v1:
time: 49.2 us; the launch traced here: 49 us
  Pallas kernels  42 us (85%)
  local copies, waits for them, and re-layouts  7.06 us (14%)
    pallas_call x1, Pallas kernels, shards(): pl.pallas_call(functools.partial(kernel, sp, tp, chunks, out_chunks), out...  42 us
    unnamed x8, local copies, waits for them, and re-layouts  5.73 us
    broadcast_in_dim x2, local copies, waits for them, and re-layouts, shards(): bias = jnp.pad(gate_bias, (0, 8 - heads), constant_values=4.0)[:, None]  1.33 us

profile of v1, /device:TPU:17, one launch (start us, length us, event | category | flops | bytes accessed | tf_op | source)
XLA Modules:
  0.0 49.0 jit_solution(6304865620221260031)
XLA Ops:
  0.0 0.7 %pad_bitcast_fusion = f32[8,1]{0,1:T(1,128)S(1)} fusion(f32[4]{0:T(128)} %param.12), kind=kLoop, calls=%fused_computation | loop fusion | bytes 48 | tf_op jit(solution)/shard_map/broadcast_in_dim | solution.py:323
  0.7 0.7 %copy.11.bias = f32[8,1]{1,0:T(8,128)} copy(f32[8,1]{0,1:T(1,128)S(1)} %pad_bitcast_fusion) | data formatting | bytes 64 | tf_op jit(solution)/shard_map/broadcast_in_dim | solution.py:323
  1.3 0.0 copy-start
  1.3 2.0 %copy.8.w_key = bf16[2048,64]{1,0:T(8,128)(2,1)} copy(bf16[2048,64]{0,1:T(8,128)(2,1)} %param.9) | data formatting | bytes 524288 | tf_op args[2]
  3.3 0.0 copy-done
  3.3 0.0 copy-start.1
  3.3 1.0 %copy.9.w_value = bf16[2048,64]{1,0:T(8,128)(2,1)} copy(bf16[2048,64]{0,1:T(8,128)(2,1)S(1)} %copy-done) | data formatting | bytes 524288 | tf_op args[3]
  4.3 0.0 copy-done.1
  4.3 1.1 %copy.10.w_gate = bf16[2048,4]{1,0:T(8,128)(2,1)} copy(bf16[2048,4]{0,1:T(4,128)(2,1)S(1)} %copy-done.1) | data formatting | bytes 32768 | tf_op args[4]
  5.4 42.0 %shard_map.73 = bf16[64,2048]{1,0:T(8,128)(2,1)} custom-call(bf16[64,2048]{1,0:T(8,128)(2,1)} %tokens.1, bf16[2048,256]{1,0:T(8,128)(2,1)} %w_query.1, bf16[2048,64]{1,0:T(8,128)(2,1)} %copy.8.w_key, bf16[2048,64]{1,0:T(8,128)(2,1)} %copy.9.w_value, bf16[2048,4]{1,0:T(8,128)(2,1)} %copy.10.w_gate, f32[8,1]{1,0:T(8,128)} %copy.11.bias, bf16[256,2048]{1,0:T(8,128)(2,1)} %w_output.1), custom_call_target="tpu_custom_call" | custom-call | tf_op jit(solution)/shard_map/pallas_call | solution.py:328
  47.4 1.7 %copy.13 = bf16[64,2048]{1,0:T(8,128)(2,1)} copy(bf16[64,2048]{1,0:T(8,128)(2,1)} %shard_map.73) | data formatting | bytes 524288
Async XLA Ops:
  1.3 2.0 %copy-start = (bf16[2048,64]{0,1:T(8,128)(2,1)S(1)}, bf16[2048,64]{0,1:T(8,128)(2,1)}, u32[]{:S(2)}) copy-start(bf16[2048,64]{0,1:T(8,128)(2,1)} %param.10) | copy-start | bytes 786436
  3.3 1.0 %copy-start.1 = (bf16[2048,4]{0,1:T(4,128)(2,1)S(1)}, bf16[2048,4]{0,1:T(4,128)(2,1)}, u32[]{:S(2)}) copy-start(bf16[2048,4]{0,1:T(4,128)(2,1)} %param.11) | copy-start | bytes 49156

commit v2 on v1

--- a/solution.py
+++ b/solution.py
@@ -17,10 +17,11 @@
     sp, tp, chunks, out_chunks,
     tokens, w_query, w_key, w_value, w_gate, bias, w_output,
     out,
-    tok, w_all, w_k, w_v, w_g, wo, wo_pair, proj, qs, kv, cum,
+    tok, w_all, w_kv, w_g, wo, wo_pair, proj, logits, qs, kv, cum, own_sum, pair_sum,
     peak, mass, accum, att, att_pair, keep, outgoing, incoming,
     local_sem, own_sem, cross_send, cross_recv, pair_send, pair_recv, relay_send, relay_recv,
     wo_send, wo_recv, kv_send, kv_recv, cum_send, cum_recv,
+    kv_side, cum_side, sum_send, sum_recv,
     att_send, att_recv, out_send, out_recv,
 ):
     lo_n = 2
@@ -33,8 +34,12 @@
     local_rows = rows * tp
     width = tok.shape[2]
     q_cols = w_query.shape[1]
-    heads = w_gate.shape[1]
-    key_cols = w_key.shape[1]
+    heads = w_gate.shape[0]
+    key_cols = w_key.shape[0]
+    span_n = 2
+    far_n = sp // span_n
+    far, side = lax.div(me, span_n), lax.rem(me, span_n)
+    mate = far * span_n + (1 - side)
     piece = width // chunks
     out_cols = w_output.shape[1]
     out_piece = out_cols // out_chunks
@@ -43,8 +48,8 @@
         return lax.rem(hi + d, hi_n) * lo_n + lo
 
     loads = [
-        pltpu.make_async_copy(w_key, w_k, local_sem.at[0]),
-        pltpu.make_async_copy(w_value, w_v, local_sem.at[1]),
+        pltpu.make_async_copy(w_key, w_kv.at[pl.ds(0, key_cols)], local_sem.at[0]),
+        pltpu.make_async_copy(w_value, w_kv.at[pl.ds(key_cols, key_cols)], local_sem.at[1]),
         pltpu.make_async_copy(w_gate, w_g, local_sem.at[2]),
         pltpu.make_async_copy(w_query, w_all.at[:, pl.ds(0, q_cols)], local_sem.at[3]),
         pltpu.make_async_copy(w_output, wo, local_sem.at[4]),
@@ -60,13 +65,13 @@
         pl.semaphore_signal(barrier, inc=1, device_id={"tp": cross(d)}, device_id_type=MESH)
 
     def greet(d, carry):
-        pl.semaphore_signal(
-            barrier, inc=1, device_id={"sp": lax.rem(me + d, sp)}, device_id_type=MESH
-        )
+        other = lax.rem(far + d, far_n) * span_n + side
+        pl.semaphore_signal(barrier, inc=1, device_id={"sp": other}, device_id_type=MESH)
         return carry
 
-    lax.fori_loop(1, sp, greet, 0)
-    pl.semaphore_wait(barrier, 1 + (hi_n - 1) + (sp - 1))
+    lax.fori_loop(1, far_n, greet, 0)
+    pl.semaphore_signal(barrier, inc=1, device_id={"sp": mate}, device_id_type=MESH)
+    pl.semaphore_wait(barrier, 1 + (hi_n - 1) + (far_n - 1) + 1)
 
     def cols(k):
         return pl.ds(k * piece, piece)
@@ -105,10 +110,7 @@
 
     def assemble(i, carry):
         span = pl.ds(pl.multiple_of(i * build, build), build)
-        w_all[span, q_cols:q_cols + LANES] = jnp.concatenate([w_k[span, :], w_v[span, :]], axis=1)
-        w_all[span, q_cols + LANES:] = jnp.concatenate(
-            [w_g[span, :], jnp.zeros((build, LANES - heads), jnp.bfloat16)], axis=1
-        )
+        w_all[span, q_cols:] = w_kv[:, span].T
         return carry
 
     lax.fori_loop(0, width // build, assemble, 0)
@@ -128,10 +130,16 @@
             relay_copy(d, k).wait_recv()
         here = tok[:, :, k * piece:(k + 1) * piece].reshape(local_rows, piece)
         part = jnp.dot(here, w_all[k * piece:(k + 1) * piece, :], preferred_element_type=jnp.float32)
+        gate_part = lax.dot_general(
+            w_g[:, k * piece:(k + 1) * piece], here, (((1,), (1,)), ((), ())),
+            preferred_element_type=jnp.float32,
+        )
         if k == 0:
             proj[...] = part
+            logits[0:heads, :] = gate_part
         else:
             proj[...] += part
+            logits[0:heads, :] += gate_part
     wo_copy.start()
 
     kv[me] = proj[:, q_cols:q_cols + 2 * key_cols].astype(jnp.bfloat16)
@@ -140,44 +148,46 @@
         q = proj[:, h * HEAD:(h + 1) * HEAD].astype(jnp.bfloat16) * jnp.bfloat16(scale)
         qs[h] = jnp.concatenate([q, jnp.zeros((local_rows, LANES - HEAD), jnp.bfloat16)], axis=1)
 
-    def kv_copy(d):
-        return pltpu.make_async_remote_copy(
-            kv.at[me], kv.at[me], kv_send.at[d], kv_recv.at[me],
-            device_id={"sp": d}, device_id_type=MESH,
-        )
-
-    def cum_copy(d):
-        return pltpu.make_async_remote_copy(
-            cum.at[me], cum.at[me], cum_send.at[d], cum_recv.at[me],
-            device_id={"sp": d}, device_id_type=MESH,
-        )
-
-    def arrival(r):
+    def column(d):
         return (
             pltpu.make_async_remote_copy(
-                kv.at[r], kv.at[r], kv_send.at[r], kv_recv.at[r],
-                device_id={"sp": r}, device_id_type=MESH,
+                kv.at[me], kv.at[me], kv_send.at[d], kv_recv.at[me],
+                device_id={"sp": d * span_n + side}, device_id_type=MESH,
             ),
             pltpu.make_async_remote_copy(
-                cum.at[r], cum.at[r], cum_send.at[r], cum_recv.at[r],
-                device_id={"sp": r}, device_id_type=MESH,
+                cum.at[me], cum.at[me], cum_send.at[d], cum_recv.at[me],
+                device_id={"sp": d * span_n + side}, device_id_type=MESH,
             ),
         )
 
-    later = sp - 1 - me
-
-    def send_kv(i, carry):
-        kv_copy(sp - 1 - i).start()
+    def across(r):
+        return (
+            pltpu.make_async_remote_copy(
+                kv.at[r], kv.at[r], kv_side.at[lax.div(r, span_n)], kv_recv.at[r],
+                device_id={"sp": mate}, device_id_type=MESH,
+            ),
+            pltpu.make_async_remote_copy(
+                cum.at[r], cum.at[r], cum_side.at[lax.div(r, span_n)], cum_recv.at[r],
+                device_id={"sp": mate}, device_id_type=MESH,
+            ),
+        )
+
+    later = far_n - 1 - far
+
+    def send_column(which, i, carry):
+        column(far_n - 1 - i)[which].start()
         return carry
 
-    def send_cum(i, carry):
-        cum_copy(sp - 1 - i).start()
-        return carry
-
-    lax.fori_loop(0, later, send_kv, 0)
-
-    logits = proj[:, q_cols + LANES:].astype(jnp.bfloat16).astype(jnp.float32).T[:8, :]
-    u = logits + bias[...]
+    lax.fori_loop(0, later, functools.partial(send_column, 0), 0)
+
+    @pl.when(side == 0)
+    def _():
+        across(me)[0].start()
+
+    row_of = lax.broadcasted_iota(jnp.int32, (8, local_rows), 0)
+    u = jnp.where(row_of < heads, logits[...].astype(jnp.bfloat16).astype(jnp.float32), 0.0)
+    for h in range(heads):
+        u = jnp.where(row_of == h, u + bias[h], u)
     gates = jnp.minimum(u, 0.0) - jnp.log1p(jnp.exp(-jnp.abs(u)))
     upper = (
         lax.broadcasted_iota(jnp.int32, (local_rows, local_rows), 0)
@@ -191,8 +201,22 @@
     total = jnp.dot(g2, ones, preferred_element_type=jnp.float32)
     total = total + jnp.dot(g1, ones, preferred_element_type=jnp.float32)
     total = total + jnp.dot(g0, ones, preferred_element_type=jnp.float32)
-    cum[me] = total
-    lax.fori_loop(0, later, send_cum, 0)
+    own_sum[...] = jnp.broadcast_to(total[:, local_rows - 1:], (8, LANES))
+    sum_copy = pltpu.make_async_remote_copy(
+        own_sum, pair_sum, sum_send, sum_recv, device_id={"sp": mate}, device_id_type=MESH
+    )
+    sum_copy.start()
+    sum_copy.wait_recv()
+    other_sum = pair_sum[...]
+    start = jnp.where(side == 1, other_sum[:, :1], 0.0)
+    total = total + start
+    cum[me, :, 0:local_rows] = total
+    cum[me, :, local_rows:] = own_sum[...] + other_sum
+    lax.fori_loop(0, later, functools.partial(send_column, 1), 0)
+
+    @pl.when(side == 0)
+    def _():
+        across(me)[1].start()
 
     halves = local_rows // LANES
 
@@ -231,19 +255,40 @@
     for h in range(heads):
         attend(h, kv[me], -total[h:h + 1, :], True)
 
-    def one_block(i, base):
-        r = me - 1 - i
-        for copy in arrival(r):
-            copy.wait_recv()
-        cum_here = cum[r]
-        base = base + cum_here[:, local_rows - 1:]
-        shift = base - cum_here
+    def block_of(r, base):
         kv_here = kv[r]
+        shift = base - cum[r, :, 0:local_rows]
         for h in range(heads):
             attend(h, kv_here, shift[h:h + 1, :], False)
+
+    def same_side(i, base):
+        r = (far - 1 - i) * span_n + side
+        for copy in across(r):
+            copy.wait_recv()
+        for copy in across(r):
+            copy.start()
+        base = base + cum[r, :, local_rows:local_rows + 1]
+        block_of(r, base)
         return base
 
-    lax.fori_loop(0, me, one_block, jnp.zeros((8, 1), jnp.float32))
+    zero = jnp.zeros((8, 1), jnp.float32)
+    lax.fori_loop(0, far, same_side, zero)
+
+    @pl.when(side == 1)
+    def _():
+        for copy in across(mate):
+            copy.wait_recv()
+        block_of(mate, zero)
+
+    def other_side(i, base):
+        r = (far - 1 - i) * span_n + 1 - side
+        for copy in across(r):
+            copy.wait_recv()
+        base = base + cum[r, :, local_rows:local_rows + 1]
+        block_of(r, base)
+        return base
+
+    lax.fori_loop(0, far, other_side, zero)
 
     for h in range(heads):
         denominator = jnp.sum(mass[h], axis=1, keepdims=True)
@@ -301,12 +346,26 @@
         for d in range(1, hi_n):
             out_copy(d, k).wait_send()
 
+    sum_copy.wait_send()
+
+    @pl.when(side == 0)
+    def _():
+        for copy in across(me):
+            copy.wait_send()
+
     def drain(i, carry):
-        kv_copy(sp - 1 - i).wait_send()
-        cum_copy(sp - 1 - i).wait_send()
+        for copy in column(far_n - 1 - i):
+            copy.wait_send()
         return carry
 
     lax.fori_loop(0, later, drain, 0)
+
+    def drain_side(i, carry):
+        for copy in across((far - 1 - i) * span_n + side):
+            copy.wait_send()
+        return carry
+
+    lax.fori_loop(0, far, drain_side, 0)
 
 
 def shards(tokens, w_query, w_key, w_value, w_gate, gate_bias, w_output):
@@ -316,11 +375,10 @@
     local_rows = rows * tp
     q_cols, key_cols, heads = w_query.shape[1], w_key.shape[1], w_gate.shape[1]
     out_cols = w_output.shape[1]
-    assert tp % 2 == 0 and 2 * key_cols == LANES and key_cols == HEAD and heads <= 8
+    assert tp % 2 == 0 and sp % 2 == 0 and 2 * key_cols == LANES and key_cols == HEAD and heads <= 8
     hi_n = tp // 2
     chunks = 4
     out_chunks = 4
-    bias = jnp.pad(gate_bias, (0, 8 - heads), constant_values=4.0)[:, None]
     bf, f32 = jnp.bfloat16, jnp.float32
     dma = pltpu.SemaphoreType.DMA
     any_spec = pl.BlockSpec(memory_space=pl.ANY)
@@ -328,20 +386,22 @@
     return pl.pallas_call(
         functools.partial(kernel, sp, tp, chunks, out_chunks),
         out_shape=jax.ShapeDtypeStruct((rows, out_cols), bf),
-        in_specs=[any_spec] * 5 + [vmem_spec, any_spec],
+        in_specs=[any_spec] * 5 + [pl.BlockSpec(memory_space=pltpu.SMEM), any_spec],
         out_specs=vmem_spec,
         scratch_shapes=[
             pltpu.VMEM((tp, rows, width), bf),
-            pltpu.VMEM((width, q_cols + 2 * LANES), bf),
-            pltpu.VMEM(w_key.shape, bf),
-            pltpu.VMEM(w_value.shape, bf),
-            pltpu.VMEM(w_gate.shape, bf),
+            pltpu.VMEM((width, q_cols + LANES), bf),
+            pltpu.VMEM((LANES, width), bf),
+            pltpu.VMEM((heads, width), bf),
             pltpu.VMEM(w_output.shape, bf),
             pltpu.VMEM(w_output.shape, bf),
-            pltpu.VMEM((local_rows, q_cols + 2 * LANES), f32),
+            pltpu.VMEM((local_rows, q_cols + LANES), f32),
+            pltpu.VMEM((8, local_rows), f32),
             pltpu.VMEM((heads, local_rows, LANES), bf),
             pltpu.VMEM((sp, local_rows, LANES), bf),
-            pltpu.VMEM((sp, 8, local_rows), f32),
+            pltpu.VMEM((sp, 8, local_rows + LANES), f32),
+            pltpu.VMEM((8, LANES), f32),
+            pltpu.VMEM((8, LANES), f32),
             pltpu.VMEM((heads, local_rows, LANES), f32),
             pltpu.VMEM((heads, local_rows, LANES), f32),
             pltpu.VMEM((heads, local_rows, LANES), f32),
@@ -360,19 +420,23 @@
             dma((hi_n - 1, chunks)),
             dma,
             dma,
+            dma((sp // 2,)),
             dma((sp,)),
+            dma((sp // 2,)),
             dma((sp,)),
-            dma((sp,)),
-            dma((sp,)),
+            dma((sp // 2,)),
+            dma((sp // 2,)),
+            dma,
+            dma,
             dma((hi_n,)),
             dma((hi_n,)),
             dma((hi_n - 1, out_chunks)),
             dma((hi_n - 1, out_chunks)),
         ],
         compiler_params=pltpu.CompilerParams(
-            collective_id=0, has_side_effects=True, vmem_limit_bytes=56 * 1024 * 1024
+            collective_id=0, has_side_effects=True, vmem_limit_bytes=(20 << 20) + (sp << 17)
         ),
-    )(tokens, w_query, w_key, w_value, w_gate, bias, w_output)
+    )(tokens, w_query, w_key.T, w_value.T, w_gate.T, gate_bias, w_output)
 
 
 def solution(mesh):

time: 49.2 us -> 44.7 us (0.909)
  Pallas kernels: 42 us -> 37 us
    pallas_call x1, Pallas kernels: 42 us -> 37 us  [shards(): pl.pallas_call(functools.partial(kernel, sp, tp, chunks, out_chunks), out...]
    unnamed x8 -> x15, local copies, waits for them, and re-layouts: 5.73 us -> 7.37 us
    broadcast_in_dim x2 -> x0, local copies, waits for them, and re-layouts: 1.33 us -> none  [shards(): bias = jnp.pad(gate_bias, (0, 8 - heads), constant_values=4.0)[:, None]]
where the time goes in v2:
time: 44.7 us; the launch traced here: 44.4 us
  Pallas kernels  37 us (83%)
  local copies, waits for them, and re-layouts  7.37 us (16%)
    pallas_call x1, Pallas kernels, shards(): pl.pallas_call(functools.partial(kernel, sp, tp, chunks, out_chunks), out...  37 us
    unnamed x15, local copies, waits for them, and re-layouts  7.37 us

profile of v2, /device:TPU:17, one launch (start us, length us, event | category | flops | bytes accessed | tf_op | source)
XLA Modules:
  0.0 44.4 jit_solution(4958644125407435745)
XLA Ops:
  0.0 0.0 copy-start.6
  0.0 0.7 %copy-done.6 = f32[4]{0:T(128)S(1)} copy-done((f32[4]{0:T(128)S(1)}, f32[4]{0:T(128)}, u32[]{:S(2)}) %copy-start.6) | copy-done | bytes 40
  0.7 0.0 copy-start
  0.7 1.2 %copy-done = bf16[2048,256]{1,0:T(8,128)(2,1)S(1)} copy-done((bf16[2048,256]{1,0:T(8,128)(2,1)S(1)}, bf16[2048,256]{1,0:T(8,128)(2,1)}, u32[]{:S(2)}) %copy-start) | copy-done | bytes 1048600
  1.9 0.0 copy-start.1
  1.9 1.2 %copy-done.1 = bf16[256,2048]{1,0:T(8,128)(2,1)S(1)} copy-done((bf16[256,2048]{1,0:T(8,128)(2,1)S(1)}, bf16[256,2048]{1,0:T(8,128)(2,1)}, u32[]{:S(2)}) %copy-start.1) | copy-done | bytes 1048600
  3.1 0.0 copy-start.2
  3.1 0.9 %copy-done.2 = bf16[64,2048]{1,0:T(8,128)(2,1)S(1)} copy-done((bf16[64,2048]{1,0:T(8,128)(2,1)S(1)}, bf16[64,2048]{1,0:T(8,128)(2,1)}, u32[]{:S(2)}) %copy-start.2) | copy-done | bytes 262168
  4.1 0.0 copy-start.3
  4.1 0.9 %copy-done.3 = bf16[2048,64]{0,1:T(8,128)(2,1)S(1)} copy-done((bf16[2048,64]{0,1:T(8,128)(2,1)S(1)}, bf16[2048,64]{0,1:T(8,128)(2,1)}, u32[]{:S(2)}) %copy-start.3) | copy-done | bytes 262168
  5.0 0.0 copy-start.4
  5.0 0.9 %copy-done.4 = bf16[2048,64]{0,1:T(8,128)(2,1)S(1)} copy-done((bf16[2048,64]{0,1:T(8,128)(2,1)S(1)}, bf16[2048,64]{0,1:T(8,128)(2,1)}, u32[]{:S(2)}) %copy-start.4) | copy-done | bytes 262168
  6.0 0.0 copy-start.5
  6.0 0.7 %copy-done.5 = bf16[2048,4]{0,1:T(4,128)(2,1)S(1)} copy-done((bf16[2048,4]{0,1:T(4,128)(2,1)S(1)}, bf16[2048,4]{0,1:T(4,128)(2,1)}, u32[]{:S(2)}) %copy-start.5) | copy-done | bytes 16408
  6.7 37.0 %shard_map.73 = bf16[64,2048]{1,0:T(8,128)(2,1)S(1)} custom-call(bf16[64,2048]{1,0:T(8,128)(2,1)S(1)} %copy-done.2, bf16[2048,256]{1,0:T(8,128)(2,1)S(1)} %copy-done, bf16[64,2048]{1,0:T(8,128)(2,1)S(1)} %bitcast.3, bf16[64,2048]{1,0:T(8,128)(2,1)S(1)} %bitcast.4, bf16[4,2048]{1,0:T(4,128)(2,1)S(1)} %bitcast.5, f32[4]{0:T(128)S(1)} %copy-done.6, ...), custom_call_target="tpu_custom_call" | custom-call | tf_op jit(solution)/shard_map/pallas_call | solution.py:386
  43.7 0.7 %copy.9 = bf16[64,2048]{1,0:T(8,128)(2,1)} copy(bf16[64,2048]{1,0:T(8,128)(2,1)S(1)} %shard_map.73) | data formatting | bytes 524288
Async XLA Ops:
  0.0 0.7 %copy-start.6 = (f32[4]{0:T(128)S(1)}, f32[4]{0:T(128)}, u32[]{:S(2)}) copy-start(f32[4]{0:T(128)} %bias.1) | copy-start | bytes 52
  0.7 1.2 %copy-start = (bf16[2048,256]{1,0:T(8,128)(2,1)S(1)}, bf16[2048,256]{1,0:T(8,128)(2,1)}, u32[]{:S(2)}) copy-start(bf16[2048,256]{1,0:T(8,128)(2,1)} %w_query.1) | copy-start | bytes 3145732
  1.9 1.2 %copy-start.1 = (bf16[256,2048]{1,0:T(8,128)(2,1)S(1)}, bf16[256,2048]{1,0:T(8,128)(2,1)}, u32[]{:S(2)}) copy-start(bf16[256,2048]{1,0:T(8,128)(2,1)} %w_output.1) | copy-start | bytes 3145732
  3.1 0.9 %copy-start.2 = (bf16[64,2048]{1,0:T(8,128)(2,1)S(1)}, bf16[64,2048]{1,0:T(8,128)(2,1)}, u32[]{:S(2)}) copy-start(bf16[64,2048]{1,0:T(8,128)(2,1)} %tokens.1) | copy-start | bytes 786436
  4.1 0.9 %copy-start.3 = (bf16[2048,64]{0,1:T(8,128)(2,1)S(1)}, bf16[2048,64]{0,1:T(8,128)(2,1)}, u32[]{:S(2)}) copy-start(bf16[2048,64]{0,1:T(8,128)(2,1)} %param.9) | copy-start | bytes 786436
  5.0 0.9 %copy-start.4 = (bf16[2048,64]{0,1:T(8,128)(2,1)S(1)}, bf16[2048,64]{0,1:T(8,128)(2,1)}, u32[]{:S(2)}) copy-start(bf16[2048,64]{0,1:T(8,128)(2,1)} %param.10) | copy-start | bytes 786436
  6.0 0.7 %copy-start.5 = (bf16[2048,4]{0,1:T(4,128)(2,1)S(1)}, bf16[2048,4]{0,1:T(4,128)(2,1)}, u32[]{:S(2)}) copy-start(bf16[2048,4]{0,1:T(4,128)(2,1)} %param.11) | copy-start | bytes 49156

commit v3 on v2

--- a/solution.py
+++ b/solution.py
@@ -15,10 +15,10 @@
 
 def kernel(
     sp, tp, chunks, out_chunks,
-    tokens, w_query, w_key, w_value, w_gate, bias, w_output,
+    tokens, w_query, w_key, w_value, w_gate, bias_in, w_output,
     out,
     tok, w_all, w_kv, w_g, wo, wo_pair, proj, logits, qs, kv, cum, own_sum, pair_sum,
-    peak, mass, accum, att, att_pair, keep, outgoing, incoming,
+    peak, mass, accum, att, att_pair, keep, outgoing, incoming, bias,
     local_sem, own_sem, cross_send, cross_recv, pair_send, pair_recv, relay_send, relay_recv,
     wo_send, wo_recv, kv_send, kv_recv, cum_send, cum_recv,
     kv_side, cum_side, sum_send, sum_recv,
@@ -43,6 +43,7 @@
     piece = width // chunks
     out_cols = w_output.shape[1]
     out_piece = out_cols // out_chunks
+    group = lo_n * rows
 
     def cross(d):
         return lax.rem(hi + d, hi_n) * lo_n + lo
@@ -53,6 +54,7 @@
         pltpu.make_async_copy(w_gate, w_g, local_sem.at[2]),
         pltpu.make_async_copy(w_query, w_all.at[:, pl.ds(0, q_cols)], local_sem.at[3]),
         pltpu.make_async_copy(w_output, wo, local_sem.at[4]),
+        pltpu.make_async_copy(bias_in, bias, local_sem.at[5]),
     ]
     own = pltpu.make_async_copy(tokens, tok.at[t_me], own_sem)
     own.start()
@@ -116,6 +118,7 @@
     lax.fori_loop(0, width // build, assemble, 0)
     loads[3].wait()
     loads[4].wait()
+    loads[5].wait()
     own.wait()
     wo_copy = pltpu.make_async_remote_copy(
         wo, wo_pair, wo_send, wo_recv, device_id={"tp": pair}, device_id_type=MESH
@@ -146,7 +149,9 @@
     scale = HEAD ** -0.5
     for h in range(heads):
         q = proj[:, h * HEAD:(h + 1) * HEAD].astype(jnp.bfloat16) * jnp.bfloat16(scale)
-        qs[h] = jnp.concatenate([q, jnp.zeros((local_rows, LANES - HEAD), jnp.bfloat16)], axis=1)
+        q = jnp.concatenate([q, jnp.zeros((local_rows, LANES - HEAD), jnp.bfloat16)], axis=1)
+        for g in range(hi_n):
+            qs[g, h * group:(h + 1) * group, :] = q[g * group:(g + 1) * group]
 
     def column(d):
         return (
@@ -206,129 +211,143 @@
         own_sum, pair_sum, sum_send, sum_recv, device_id={"sp": mate}, device_id_type=MESH
     )
     sum_copy.start()
-    sum_copy.wait_recv()
-    other_sum = pair_sum[...]
-    start = jnp.where(side == 1, other_sum[:, :1], 0.0)
-    total = total + start
-    cum[me, :, 0:local_rows] = total
-    cum[me, :, local_rows:] = own_sum[...] + other_sum
-    lax.fori_loop(0, later, functools.partial(send_column, 1), 0)
-
-    @pl.when(side == 0)
-    def _():
-        across(me)[1].start()
 
     halves = local_rows // LANES
 
     def lane_parts(x):
         return [x[:, j * LANES:(j + 1) * LANES] for j in range(halves)]
 
-    def attend(h, kv_here, bias_row, first):
+    def attend(g, kv_here, shift, first):
         s = lax.dot_general(
-            qs[h], kv_here, (((1,), (1,)), ((), ())), preferred_element_type=jnp.float32
-        ) + bias_row
-        if first:
-            allowed = (
-                lax.broadcasted_iota(jnp.int32, (local_rows, local_rows), 1)
-                <= lax.broadcasted_iota(jnp.int32, (local_rows, local_rows), 0)
-            )
-            s = jnp.where(allowed, s, masked_value)
-        top = jnp.max(s, axis=1, keepdims=True)
-        if first:
-            new_peak = jnp.broadcast_to(top, (local_rows, LANES))
-        else:
-            old_peak = peak[h]
-            new_peak = jnp.maximum(old_peak, top)
-        p = [jnp.exp(x - new_peak) for x in lane_parts(s)]
-        p_sum = functools.reduce(lambda a, b: a + b, p)
-        weights = jnp.concatenate([x.astype(jnp.bfloat16) for x in p], axis=1)
-        term = jnp.dot(weights, kv_here, preferred_element_type=jnp.float32)
-        peak[h] = new_peak
-        if first:
-            mass[h] = p_sum
-            accum[h] = term
-        else:
-            rescale = jnp.exp(old_peak - new_peak)
-            mass[h] = mass[h] * rescale + p_sum
-            accum[h] = accum[h] * rescale + term
-
-    for h in range(heads):
-        attend(h, kv[me], -total[h:h + 1, :], True)
-
-    def block_of(r, base):
-        kv_here = kv[r]
-        shift = base - cum[r, :, 0:local_rows]
+            qs[g], kv_here, (((1,), (1,)), ((), ())), preferred_element_type=jnp.float32
+        )
+        weights = []
+        rescales = []
         for h in range(heads):
-            attend(h, kv_here, shift[h:h + 1, :], False)
-
-    def same_side(i, base):
-        r = (far - 1 - i) * span_n + side
-        for copy in across(r):
-            copy.wait_recv()
-        for copy in across(r):
-            copy.start()
-        base = base + cum[r, :, local_rows:local_rows + 1]
-        block_of(r, base)
-        return base
-
-    zero = jnp.zeros((8, 1), jnp.float32)
-    lax.fori_loop(0, far, same_side, zero)
-
-    @pl.when(side == 1)
-    def _():
-        for copy in across(mate):
-            copy.wait_recv()
-        block_of(mate, zero)
-
-    def other_side(i, base):
-        r = (far - 1 - i) * span_n + 1 - side
-        for copy in across(r):
-            copy.wait_recv()
-        base = base + cum[r, :, local_rows:local_rows + 1]
-        block_of(r, base)
-        return base
-
-    lax.fori_loop(0, far, other_side, zero)
-
-    for h in range(heads):
-        denominator = jnp.sum(mass[h], axis=1, keepdims=True)
-        done = (accum[h][:, key_cols:2 * key_cols] / denominator).astype(jnp.bfloat16)
-        att[:, :, :, h * HEAD:(h + 1) * HEAD] = done.reshape(hi_n, lo_n, rows, HEAD)
-
-    def att_copy(d):
+            here = slice(h * group, (h + 1) * group)
+            x = s[here] + shift[h:h + 1, :]
+            if first:
+                allowed = (
+                    lax.broadcasted_iota(jnp.int32, (group, local_rows), 1)
+                    <= lax.broadcasted_iota(jnp.int32, (group, local_rows), 0) + g * group
+                )
+                x = jnp.where(allowed, x, masked_value)
+            top = jnp.max(x, axis=1, keepdims=True)
+            if first:
+                new_peak = jnp.broadcast_to(top, (group, LANES))
+            else:
+                old_peak = peak[here, :]
+                new_peak = jnp.maximum(old_peak, top)
+                rescale = jnp.exp(old_peak - new_peak)
+                rescales.append(rescale)
+            p = [jnp.exp(part - new_peak) for part in lane_parts(x)]
+            p_sum = functools.reduce(lambda a, b: a + b, p)
+            weights.append(jnp.concatenate([part.astype(jnp.bfloat16) for part in p], axis=1))
+            peak[here, :] = new_peak
+            mass[here, :] = p_sum if first else mass[here, :] * rescale + p_sum
+        term = jnp.dot(
+            jnp.concatenate(weights, axis=0), kv_here, preferred_element_type=jnp.float32
+        )
+        for h in range(heads):
+            here = slice(h * group, (h + 1) * group)
+            if first:
+                accum[here, :] = term[here]
+            else:
+                accum[here, :] = accum[here, :] * rescales[h] + term[here]
+
+    def pass_over(g, fresh):
+        attend(g, kv[me], -total, True)
+        if fresh:
+            sum_copy.wait_recv()
+            start = jnp.where(side == 1, pair_sum[:, :1], 0.0)
+            cum[me, :, 0:local_rows] = total + start
+            cum[me, :, local_rows:] = own_sum[...] + pair_sum[...]
+            lax.fori_loop(0, later, functools.partial(send_column, 1), 0)
+
+            @pl.when(side == 0)
+            def _():
+                across(me)[1].start()
+
+        start = jnp.where(side == 1, pair_sum[:, :1], 0.0)
+
+        def same_side(i, base):
+            r = (far - 1 - i) * span_n + side
+            if fresh:
+                for copy in across(r):
+                    copy.wait_recv()
+                for copy in across(r):
+                    copy.start()
+            base = base + cum[r, :, local_rows:local_rows + 1]
+            attend(g, kv[r], base - cum[r, :, 0:local_rows], False)
+            return base
+
+        lax.fori_loop(0, far, same_side, start)
+
+        @pl.when(side == 1)
+        def _():
+            if fresh:
+                for copy in across(mate):
+                    copy.wait_recv()
+            attend(g, kv[mate], start - cum[mate, :, 0:local_rows], False)
+
+        def other_side(i, base):
+            r = (far - 1 - i) * span_n + 1 - side
+            if fresh:
+                for copy in across(r):
+                    copy.wait_recv()
+            base = base + cum[r, :, local_rows:local_rows + 1]
+            attend(g, kv[r], base - cum[r, :, 0:local_rows], False)
+            return base
+
+        lax.fori_loop(0, far, other_side, start)
+
+        for h in range(heads):
+            here = slice(h * group, (h + 1) * group)
+            denominator = jnp.sum(mass[here, :], axis=1, keepdims=True)
+            done = (accum[here, key_cols:2 * key_cols] / denominator).astype(jnp.bfloat16)
+            att[g, :, :, h * HEAD:(h + 1) * HEAD] = done.reshape(lo_n, rows, HEAD)
+
+    def att_copy(g):
         return pltpu.make_async_remote_copy(
-            att.at[d, 1 - lo], att_pair.at[d], att_send.at[d], att_recv.at[d],
+            att.at[g, 1 - lo], att_pair.at[g], att_send.at[g], att_recv.at[g],
             device_id={"tp": pair}, device_id_type=MESH,
         )
-
-    for d in range(hi_n):
-        att_copy(d).start()
-    wo_copy.wait_recv()
-    for d in range(hi_n):
-        att_copy(d).wait_recv()
-    mine = att[:, lo].reshape(hi_n * rows, q_cols)
-    theirs = att_pair[...].reshape(hi_n * rows, q_cols)
 
     def out_copy(d, k):
         span = pl.ds(k * out_piece, out_piece)
         return pltpu.make_async_remote_copy(
-            outgoing.at[lax.rem(hi + d, hi_n), :, span], incoming.at[d - 1, :, span],
+            outgoing.at[d - 1, :, span], incoming.at[d - 1, :, span],
             out_send.at[d - 1, k], out_recv.at[d - 1, k],
             device_id={"tp": cross(d)}, device_id_type=MESH,
         )
 
+    def combined(g, k):
+        span = slice(k * out_piece, (k + 1) * out_piece)
+        a = jnp.dot(att[g, lo], wo[:, span], preferred_element_type=jnp.float32)
+        b = jnp.dot(att_pair[g], wo_pair[:, span], preferred_element_type=jnp.float32)
+        return (
+            a.astype(jnp.bfloat16).astype(jnp.float32) + b.astype(jnp.bfloat16).astype(jnp.float32)
+        )
+
+    for d in list(range(1, hi_n)):
+        g = lax.rem(hi + d, hi_n)
+        pass_over(g, d == 1)
+        att_copy(g).start()
+        if d == 1:
+            wo_copy.wait_recv()
+        att_copy(g).wait_recv()
+        for k in range(out_chunks):
+            span = slice(k * out_piece, (k + 1) * out_piece)
+            outgoing[d - 1, :, span] = combined(g, k).astype(jnp.bfloat16)
+            out_copy(d, k).start()
+    pass_over(hi, False)
+    att_copy(hi).start()
+    att_copy(hi).wait_recv()
+    for k in range(out_chunks):
+        keep[:, k * out_piece:(k + 1) * out_piece] = combined(hi, k)
     for k in range(out_chunks):
         span = slice(k * out_piece, (k + 1) * out_piece)
-        a = jnp.dot(mine, wo[:, span], preferred_element_type=jnp.float32).astype(jnp.bfloat16)
-        b = jnp.dot(theirs, wo_pair[:, span], preferred_element_type=jnp.float32).astype(jnp.bfloat16)
-        both = a.astype(jnp.float32) + b.astype(jnp.float32)
-        keep[:, :, span] = both.reshape(hi_n, rows, out_piece)
-        outgoing[:, :, span] = both.astype(jnp.bfloat16).reshape(hi_n, rows, out_piece)
-        for d in range(1, hi_n):
-            out_copy(d, k).start()
-    for k in range(out_chunks):
-        span = slice(k * out_piece, (k + 1) * out_piece)
-        value = keep[hi, :, span]
+        value = keep[:, span]
         for d in range(1, hi_n):
             out_copy(d, k).wait_recv()
             value = value + incoming[d - 1, :, span].astype(jnp.float32)
@@ -375,18 +394,19 @@
     local_rows = rows * tp
     q_cols, key_cols, heads = w_query.shape[1], w_key.shape[1], w_gate.shape[1]
     out_cols = w_output.shape[1]
-    assert tp % 2 == 0 and sp % 2 == 0 and 2 * key_cols == LANES and key_cols == HEAD and heads <= 8
+    assert tp % 2 == 0 and sp % 2 == 0 and tp >= 4 and 2 * key_cols == LANES and key_cols == HEAD and heads <= 8
     hi_n = tp // 2
     chunks = 4
     out_chunks = 4
     bf, f32 = jnp.bfloat16, jnp.float32
     dma = pltpu.SemaphoreType.DMA
-    any_spec = pl.BlockSpec(memory_space=pl.ANY)
+    hbm_spec = pl.BlockSpec(memory_space=pltpu.HBM)
     vmem_spec = pl.BlockSpec(memory_space=pltpu.VMEM)
+    operands = (tokens, w_query, w_key.T, w_value.T, w_gate.T, gate_bias, w_output)
     return pl.pallas_call(
         functools.partial(kernel, sp, tp, chunks, out_chunks),
         out_shape=jax.ShapeDtypeStruct((rows, out_cols), bf),
-        in_specs=[any_spec] * 5 + [pl.BlockSpec(memory_space=pltpu.SMEM), any_spec],
+        in_specs=[hbm_spec] * 7,
         out_specs=vmem_spec,
         scratch_shapes=[
             pltpu.VMEM((tp, rows, width), bf),
@@ -397,20 +417,21 @@
             pltpu.VMEM(w_output.shape, bf),
             pltpu.VMEM((local_rows, q_cols + LANES), f32),
             pltpu.VMEM((8, local_rows), f32),
-            pltpu.VMEM((heads, local_rows, LANES), bf),
+            pltpu.VMEM((hi_n, heads * 2 * rows, LANES), bf),
             pltpu.VMEM((sp, local_rows, LANES), bf),
             pltpu.VMEM((sp, 8, local_rows + LANES), f32),
             pltpu.VMEM((8, LANES), f32),
             pltpu.VMEM((8, LANES), f32),
-            pltpu.VMEM((heads, local_rows, LANES), f32),
-            pltpu.VMEM((heads, local_rows, LANES), f32),
-            pltpu.VMEM((heads, local_rows, LANES), f32),
+            pltpu.VMEM((heads * 2 * rows, LANES), f32),
+            pltpu.VMEM((heads * 2 * rows, LANES), f32),
+            pltpu.VMEM((heads * 2 * rows, LANES), f32),
             pltpu.VMEM((hi_n, 2, rows, q_cols), bf),
             pltpu.VMEM((hi_n, rows, q_cols), bf),
-            pltpu.VMEM((hi_n, rows, out_cols), f32),
-            pltpu.VMEM((hi_n, rows, out_cols), bf),
+            pltpu.VMEM((rows, out_cols), f32),
+            pltpu.VMEM((hi_n - 1, rows, out_cols), bf),
             pltpu.VMEM((max(hi_n - 1, 1), rows, out_cols), bf),
-            dma((5,)),
+            pltpu.SMEM((heads,), f32),
+            dma((6,)),
             dma,
             dma((hi_n - 1, chunks)),
             dma((hi_n - 1, chunks)),
@@ -436,7 +457,7 @@
         compiler_params=pltpu.CompilerParams(
             collective_id=0, has_side_effects=True, vmem_limit_bytes=(20 << 20) + (sp << 17)
         ),
-    )(tokens, w_query, w_key.T, w_value.T, w_gate.T, gate_bias, w_output)
+    )(*(pltpu.with_memory_space_constraint(x, pltpu.HBM) for x in operands))
 
 
 def solution(mesh):

time: 44.7 us -> 36.7 us (0.82)
  local copies, waits for them, and re-layouts: 7.37 us -> 0.71 us
  Pallas kernels: 37 us -> 35.8 us
    unnamed x15 -> x1, local copies, waits for them, and re-layouts: 7.37 us -> 0.71 us
    pallas_call x1, Pallas kernels: 37 us -> 35.8 us  [shards(): pl.pallas_call(functools.partial(kernel, sp, tp, chunks, out_chunks), out...]
where the time goes in v3:
time: 36.7 us; the launch traced here: 36.5 us
  Pallas kernels  35.8 us (98%)
  local copies, waits for them, and re-layouts  0.71 us (2%)
    pallas_call x1, Pallas kernels, shards(): pl.pallas_call(functools.partial(kernel, sp, tp, chunks, out_chunks), out...  35.8 us

profile of v3, /device:TPU:17, one launch (start us, length us, event | category | flops | bytes accessed | tf_op | source)
XLA Modules:
  0.0 36.5 jit_solution(1292921708715656939)
XLA Ops:
  0.0 35.8 %shard_map.73 = bf16[64,2048]{1,0:T(8,128)(2,1)S(1)} custom-call(bf16[64,2048]{1,0:T(8,128)(2,1)} %tokens.1, bf16[2048,256]{1,0:T(8,128)(2,1)} %w_query.1, bf16[64,2048]{1,0:T(8,128)(2,1)} %bitcast.3, bf16[64,2048]{1,0:T(8,128)(2,1)} %bitcast.4, bf16[4,2048]{1,0:T(4,128)(2,1)} %bitcast.5, f32[4]{0:T(128)} %bias_in.1, bf16[256,2048]{1,0:T(8,128)(2,1)} %w_output.1), custom_call_target="tpu_custom_call" | custom-call | tf_op jit(solution)/shard_map/pallas_call | solution.py:406
  35.8 0.7 %copy.9 = bf16[64,2048]{1,0:T(8,128)(2,1)} copy(bf16[64,2048]{1,0:T(8,128)(2,1)S(1)} %shard_map.73) | data formatting | bytes 524288

commit v4 on v3

--- a/solution.py
+++ b/solution.py
@@ -80,14 +80,14 @@
 
     def cross_copy(d, k):
         return pltpu.make_async_remote_copy(
-            tokens.at[:, cols(k)], tok.at[t_me, :, cols(k)],
+            tok.at[t_me, :, cols(k)], tok.at[t_me, :, cols(k)],
             cross_send.at[d - 1, k], cross_recv.at[d - 1, k],
             device_id={"tp": cross(d)}, device_id_type=MESH,
         )
 
     def pair_copy(k):
         return pltpu.make_async_remote_copy(
-            tokens.at[:, cols(k)], tok.at[t_me, :, cols(k)],
+            tok.at[t_me, :, cols(k)], tok.at[t_me, :, cols(k)],
             pair_send.at[k], pair_recv.at[k],
             device_id={"tp": pair}, device_id_type=MESH,
         )
@@ -100,6 +100,7 @@
             device_id={"tp": pair}, device_id_type=MESH,
         )
 
+    own.wait()
     for k in range(chunks):
         for d in range(1, hi_n):
             cross_copy(d, k).start()
@@ -119,7 +120,6 @@
     loads[3].wait()
     loads[4].wait()
     loads[5].wait()
-    own.wait()
     wo_copy = pltpu.make_async_remote_copy(
         wo, wo_pair, wo_send, wo_recv, device_id={"tp": pair}, device_id_type=MESH
     )
@@ -144,50 +144,6 @@
             proj[...] += part
             logits[0:heads, :] += gate_part
     wo_copy.start()
-
-    kv[me] = proj[:, q_cols:q_cols + 2 * key_cols].astype(jnp.bfloat16)
-    scale = HEAD ** -0.5
-    for h in range(heads):
-        q = proj[:, h * HEAD:(h + 1) * HEAD].astype(jnp.bfloat16) * jnp.bfloat16(scale)
-        q = jnp.concatenate([q, jnp.zeros((local_rows, LANES - HEAD), jnp.bfloat16)], axis=1)
-        for g in range(hi_n):
-            qs[g, h * group:(h + 1) * group, :] = q[g * group:(g + 1) * group]
-
-    def column(d):
-        return (
-            pltpu.make_async_remote_copy(
-                kv.at[me], kv.at[me], kv_send.at[d], kv_recv.at[me],
-                device_id={"sp": d * span_n + side}, device_id_type=MESH,
-            ),
-            pltpu.make_async_remote_copy(
-                cum.at[me], cum.at[me], cum_send.at[d], cum_recv.at[me],
-                device_id={"sp": d * span_n + side}, device_id_type=MESH,
-            ),
-        )
-
-    def across(r):
-        return (
-            pltpu.make_async_remote_copy(
-                kv.at[r], kv.at[r], kv_side.at[lax.div(r, span_n)], kv_recv.at[r],
-                device_id={"sp": mate}, device_id_type=MESH,
-            ),
-            pltpu.make_async_remote_copy(
-                cum.at[r], cum.at[r], cum_side.at[lax.div(r, span_n)], cum_recv.at[r],
-                device_id={"sp": mate}, device_id_type=MESH,
-            ),
-        )
-
-    later = far_n - 1 - far
-
-    def send_column(which, i, carry):
-        column(far_n - 1 - i)[which].start()
-        return carry
-
-    lax.fori_loop(0, later, functools.partial(send_column, 0), 0)
-
-    @pl.when(side == 0)
-    def _():
-        across(me)[0].start()
 
     row_of = lax.broadcasted_iota(jnp.int32, (8, local_rows), 0)
     u = jnp.where(row_of < heads, logits[...].astype(jnp.bfloat16).astype(jnp.float32), 0.0)
@@ -211,6 +167,50 @@
         own_sum, pair_sum, sum_send, sum_recv, device_id={"sp": mate}, device_id_type=MESH
     )
     sum_copy.start()
+
+    kv[me] = proj[:, q_cols:q_cols + 2 * key_cols].astype(jnp.bfloat16)
+    scale = HEAD ** -0.5
+    for h in range(heads):
+        q = proj[:, h * HEAD:(h + 1) * HEAD].astype(jnp.bfloat16) * jnp.bfloat16(scale)
+        q = jnp.concatenate([q, jnp.zeros((local_rows, LANES - HEAD), jnp.bfloat16)], axis=1)
+        for g in range(hi_n):
+            qs[g, h * group:(h + 1) * group, :] = q[g * group:(g + 1) * group]
+
+    def column(d):
+        return (
+            pltpu.make_async_remote_copy(
+                kv.at[me], kv.at[me], kv_send.at[d], kv_recv.at[me],
+                device_id={"sp": d * span_n + side}, device_id_type=MESH,
+            ),
+            pltpu.make_async_remote_copy(
+                cum.at[me], cum.at[me], cum_send.at[d], cum_recv.at[me],
+                device_id={"sp": d * span_n + side}, device_id_type=MESH,
+            ),
+        )
+
+    def across(r):
+        return (
+            pltpu.make_async_remote_copy(
+                kv.at[r], kv.at[r], kv_side.at[lax.div(r, span_n)], kv_recv.at[r],
+                device_id={"sp": mate}, device_id_type=MESH,
+            ),
+            pltpu.make_async_remote_copy(
+                cum.at[r], cum.at[r], cum_side.at[lax.div(r, span_n)], cum_recv.at[r],
+                device_id={"sp": mate}, device_id_type=MESH,
+            ),
+        )
+
+    later = far_n - 1 - far
+
+    def send_column(which, i, carry):
+        column(far + 1 + i)[which].start()
+        return carry
+
+    lax.fori_loop(0, jnp.minimum(later, 1), functools.partial(send_column, 0), 0)
+
+    @pl.when(side == 0)
+    def _():
+        across(me)[0].start()
 
     halves = local_rows // LANES
 
@@ -263,6 +263,7 @@
             cum[me, :, 0:local_rows] = total + start
             cum[me, :, local_rows:] = own_sum[...] + pair_sum[...]
             lax.fori_loop(0, later, functools.partial(send_column, 1), 0)
+            lax.fori_loop(1, later, functools.partial(send_column, 0), 0)
 
             @pl.when(side == 0)
             def _():
@@ -396,8 +397,8 @@
     out_cols = w_output.shape[1]
     assert tp % 2 == 0 and sp % 2 == 0 and tp >= 4 and 2 * key_cols == LANES and key_cols == HEAD and heads <= 8
     hi_n = tp // 2
-    chunks = 4
-    out_chunks = 4
+    chunks = 8
+    out_chunks = 8
     bf, f32 = jnp.bfloat16, jnp.float32
     dma = pltpu.SemaphoreType.DMA
     hbm_spec = pl.BlockSpec(memory_space=pltpu.HBM)

time: 36.7 us -> 39.2 us (1.068)
  the two profiles are of different devices: /device:TPU:17 before, /device:TPU:27 now
where the time goes in v4:
time: 39.2 us; the launch traced here: 39 us
  Pallas kernels  38.3 us (98%)
  local copies, waits for them, and re-layouts  0.71 us (2%)
    pallas_call x1, Pallas kernels, shards(): pl.pallas_call(functools.partial(kernel, sp, tp, chunks, out_chunks), out...  38.3 us

profile of v4, /device:TPU:27, one launch (start us, length us, event | category | flops | bytes accessed | tf_op | source)
XLA Modules:
  0.0 39.0 jit_solution(16344284049732770246)
XLA Ops:
  0.0 38.3 %shard_map.73 = bf16[64,2048]{1,0:T(8,128)(2,1)S(1)} custom-call(bf16[64,2048]{1,0:T(8,128)(2,1)} %tokens.1, bf16[2048,256]{1,0:T(8,128)(2,1)} %w_query.1, bf16[64,2048]{1,0:T(8,128)(2,1)} %bitcast.3, bf16[64,2048]{1,0:T(8,128)(2,1)} %bitcast.4, bf16[4,2048]{1,0:T(4,128)(2,1)} %bitcast.5, f32[4]{0:T(128)} %bias_in.1, bf16[256,2048]{1,0:T(8,128)(2,1)} %w_output.1), custom_call_target="tpu_custom_call" | custom-call | tf_op jit(solution)/shard_map/pallas_call | solution.py:407
  38.3 0.7 %copy.9 = bf16[64,2048]{1,0:T(8,128)(2,1)} copy(bf16[64,2048]{1,0:T(8,128)(2,1)S(1)} %shard_map.73) | data formatting | bytes 524288

commit v5 on v4

--- a/solution.py
+++ b/solution.py
@@ -44,6 +44,7 @@
     out_cols = w_output.shape[1]
     out_piece = out_cols // out_chunks
     group = lo_n * rows
+    half = 4
 
     def cross(d):
         return lax.rem(hi + d, hi_n) * lo_n + lo
@@ -260,8 +261,8 @@
         if fresh:
             sum_copy.wait_recv()
             start = jnp.where(side == 1, pair_sum[:, :1], 0.0)
-            cum[me, :, 0:local_rows] = total + start
-            cum[me, :, local_rows:] = own_sum[...] + pair_sum[...]
+            both_sums = jnp.broadcast_to((own_sum[...] + pair_sum[...])[:, :1], (8, local_rows))
+            cum[me] = jnp.concatenate([(total + start)[:half], both_sums[:half]], axis=0)
             lax.fori_loop(0, later, functools.partial(send_column, 1), 0)
             lax.fori_loop(1, later, functools.partial(send_column, 0), 0)
 
@@ -269,7 +270,7 @@
             def _():
                 across(me)[1].start()
 
-        start = jnp.where(side == 1, pair_sum[:, :1], 0.0)
+        start = jnp.where(side == 1, pair_sum[0:half, :1], 0.0)
 
         def same_side(i, base):
             r = (far - 1 - i) * span_n + side
@@ -278,8 +279,8 @@
                     copy.wait_recv()
                 for copy in across(r):
                     copy.start()
-            base = base + cum[r, :, local_rows:local_rows + 1]
-            attend(g, kv[r], base - cum[r, :, 0:local_rows], False)
+            base = base + cum[r, half:, 0:1]
+            attend(g, kv[r], base - cum[r, 0:half, :], False)
             return base
 
         lax.fori_loop(0, far, same_side, start)
@@ -289,15 +290,15 @@
             if fresh:
                 for copy in across(mate):
                     copy.wait_recv()
-            attend(g, kv[mate], start - cum[mate, :, 0:local_rows], False)
+            attend(g, kv[mate], start - cum[mate, 0:half, :], False)
 
         def other_side(i, base):
             r = (far - 1 - i) * span_n + 1 - side
             if fresh:
                 for copy in across(r):
                     copy.wait_recv()
-            base = base + cum[r, :, local_rows:local_rows + 1]
-            attend(g, kv[r], base - cum[r, :, 0:local_rows], False)
+            base = base + cum[r, half:, 0:1]
+            attend(g, kv[r], base - cum[r, 0:half, :], False)
             return base
 
         lax.fori_loop(0, far, other_side, start)
@@ -395,10 +396,10 @@
     local_rows = rows * tp
     q_cols, key_cols, heads = w_query.shape[1], w_key.shape[1], w_gate.shape[1]
     out_cols = w_output.shape[1]
-    assert tp % 2 == 0 and sp % 2 == 0 and tp >= 4 and 2 * key_cols == LANES and key_cols == HEAD and heads <= 8
+    assert tp % 2 == 0 and sp % 2 == 0 and tp >= 4 and 2 * key_cols == LANES and key_cols == HEAD and heads <= 4
     hi_n = tp // 2
-    chunks = 8
-    out_chunks = 8
+    chunks = 2
+    out_chunks = 2
     bf, f32 = jnp.bfloat16, jnp.float32
     dma = pltpu.SemaphoreType.DMA
     hbm_spec = pl.BlockSpec(memory_space=pltpu.HBM)
@@ -420,7 +421,7 @@
             pltpu.VMEM((8, local_rows), f32),
             pltpu.VMEM((hi_n, heads * 2 * rows, LANES), bf),
             pltpu.VMEM((sp, local_rows, LANES), bf),
-            pltpu.VMEM((sp, 8, local_rows + LANES), f32),
+            pltpu.VMEM((sp, 8, local_rows), f32),
             pltpu.VMEM((8, LANES), f32),
             pltpu.VMEM((8, LANES), f32),
             pltpu.VMEM((heads * 2 * rows, LANES), f32),

time: 39.2 us -> 34.9 us (0.89)
  the two profiles are of different devices: /device:TPU:27 before, /device:TPU:25 now
where the time goes in v5:
time: 34.9 us; the launch traced here: 34.7 us
  Pallas kernels  34 us (97%)
  local copies, waits for them, and re-layouts  0.71 us (2%)
    pallas_call x1, Pallas kernels, shards(): pl.pallas_call(functools.partial(kernel, sp, tp, chunks, out_chunks), out...  34 us
    unnamed x1, local copies, waits for them, and re-layouts  0.71 us

profile of v5, /device:TPU:25, one launch (start us, length us, event | category | flops | bytes accessed | tf_op | source)
XLA Modules:
  0.0 34.7 jit_solution(2468775703167878043)
XLA Ops:
  0.0 34.0 %shard_map.73 = bf16[64,2048]{1,0:T(8,128)(2,1)S(1)} custom-call(bf16[64,2048]{1,0:T(8,128)(2,1)} %tokens.1, bf16[2048,256]{1,0:T(8,128)(2,1)} %w_query.1, bf16[64,2048]{1,0:T(8,128)(2,1)} %bitcast.3, bf16[64,2048]{1,0:T(8,128)(2,1)} %bitcast.4, bf16[4,2048]{1,0:T(4,128)(2,1)} %bitcast.5, f32[4]{0:T(128)} %bias_in.1, bf16[256,2048]{1,0:T(8,128)(2,1)} %w_output.1), custom_call_target="tpu_custom_call" | custom-call | tf_op jit(solution)/shard_map/pallas_call | solution.py:408
  34.0 0.7 %copy.9 = bf16[64,2048]{1,0:T(8,128)(2,1)} copy(bf16[64,2048]{1,0:T(8,128)(2,1)S(1)} %shard_map.73) | data formatting | bytes 524288
